TPU v7x, 32 devices: a whole 2x2x4 slice. The times are simulated.
32 devices in a mesh: ep: 8 (over z, y), tp: 4 (over x, core).
Axes of the slice: x: 2, y: 2, z: 4, core: 2. Of those that a mesh axis runs over, the one named last changes fastest.
Arguments:
- queries: bfloat16 [4096, 2048], P('ep', 'tp'), may hold values from -6 to 6
- key_rows: bfloat16 [4096, 2048], P('ep', 'tp'), may hold values from -6 to 6
- value_rows: bfloat16 [4096, 4096], P('ep', 'tp'), may hold values from -6 to 6
- gate_rows: bfloat16 [4096, 4096], P('ep', 'tp'), may hold values from -6 to 6
- log_decay: float32 [16, 4096], P('tp', 'ep'), may hold values from -1 to 0
- head_gain: float32 [4096], P('tp'), may hold values from 0.1 to 1.9
- out_weight: bfloat16 [4096, 4096], P('tp'), may hold values from -0.09375 to 0.09375
- expert_input: bfloat16 [4096, 4096], P('ep'), may hold values from -6 to 6
- input_gain: float32 [4096], replicated, may hold values from 0.1 to 1.9
- route_ids: int32 [4096, 2], P('ep'), may hold values from 0 to 7, as said below
- route_weight: float32 [4096, 2], P('ep'), may hold values from 0.1 to 0.9
- expert_gate: bfloat16 [8, 4096, 1024], P('ep', None, 'tp'), may hold values from -0.09375 to 0.09375
- expert_up: bfloat16 [8, 4096, 1024], P('ep', None, 'tp'), may hold values from -0.09375 to 0.09375
- expert_down: bfloat16 [8, 1024, 4096], P('ep', 'tp'), may hold values from -0.1875 to 0.1875
Outputs:
- mixer_out: bfloat16 [4096, 4096], P(('ep', 'tp'))
- expert_out: bfloat16 [4096, 4096], P('ep', 'tp')
Inputs may be any that keep to these rules, and one draw needn't show every extreme that they name: `route_ids`: each row names two different experts of one group of 8 consecutive experts. On the rows of one device each group is named by exactly 512 rows, experts 2 i and 2 i + 1 together are named exactly 4 * 192 / 3 times, and no expert is named by more than 192 rows; one expert is named by exactly 192 rows of every device.
All inputs are finite; a program needn't handle non-finite values.
Results may differ from a plain program's by a relative error of at most 0.019.
Values may be sent and summed in bfloat16 or wider, within the bound.
A program may use at most 192 MiB of HBM per device.

v0:
```python
import jax
import jax.numpy as jnp
from jax import lax
from jax.sharding import PartitionSpec as P

BLOCK = 512
epsilon = 1e-06
theta_base = 10000.0
largest_entry = lax.Precision.HIGHEST


def prefix(value, axis, combine, identity):
    length, index = (lax.axis_size(axis), lax.axis_index(axis))
    everything = jax.tree.map(
        lambda part, kind: lax.all_gather(part.astype(kind), axis),
        value,
        (jnp.bfloat16, jnp.bfloat16),
    )
    start = jax.tree.map(
        lambda part, zero: jnp.broadcast_to(jnp.asarray(zero, part.dtype), part.shape),
        value,
        identity,
    )

    def hop(k, before):
        reached = k < index
        new = combine(
            before, jax.tree.map(lambda part, own: part[k].astype(own.dtype), everything, value)
        )
        return jax.tree.map(lambda a, b: jnp.where(reached, a, b), new, before)

    return lax.fori_loop(0, length, hop, start)


def rotate(values, positions):
    half_dim = values.shape[-1] // 2
    frequency = theta_base ** (-jnp.arange(half_dim, dtype=jnp.float32) / half_dim)
    angles = positions.astype(jnp.float32)[:, None, None] * frequency
    cosine = jnp.cos(angles)
    sine_wave = jnp.sin(angles)
    first_half = values[..., :half_dim]
    second = values[..., half_dim:]
    return jnp.concatenate(
        [first_half * cosine - second * sine_wave, second * cosine + first_half * sine_wave],
        axis=-1,
    )


def round_back(values):
    return lax.optimization_barrier(values.astype(jnp.bfloat16)).astype(jnp.float32)


def to_blocks(array, blocks):
    return array.reshape(blocks, array.shape[0] // blocks, array.shape[1], array.shape[2])


def combine_states(earlier, later):
    return (later[1][:, None, None] * earlier[0] + later[0], earlier[1] * later[1])


def retention_rows(queries, key_rows, value_rows, gate_rows, log_decay, head_gain):
    length = queries.shape[0]
    head_count = log_decay.shape[0]
    key_width = queries.shape[1] // head_count
    value_width = value_rows.shape[1] // head_count
    blocks = length // BLOCK
    positions = lax.axis_index("ep") * length + jnp.arange(length, dtype=jnp.int32)
    query_rot = to_blocks(
        rotate(queries.astype(jnp.float32).reshape(length, head_count, key_width), positions),
        blocks,
    )
    key_rot = to_blocks(
        rotate(key_rows.astype(jnp.float32).reshape(length, head_count, key_width), positions)
        * key_width ** (-0.5),
        blocks,
    )
    value_all = to_blocks(
        value_rows.astype(jnp.float32).reshape(length, head_count, value_width), blocks
    )
    running = jnp.cumsum(log_decay.reshape(head_count, blocks, BLOCK), axis=2)
    ending = running[:, :, -1]
    kept = jnp.exp(ending[:, :, None] - running)
    block_states = jnp.einsum(
        "nlhd,hnl,nlhe->nhde", key_rot, kept, value_all, precision=largest_entry
    )
    block_decay = jnp.exp(ending).T

    def advance(carried, inputs):
        decay_now, state_now = inputs
        return (decay_now[:, None, None] * carried + state_now, carried)

    zeros_state = jnp.zeros((head_count, key_width, value_width), jnp.float32)
    device_state, local_starts = lax.scan(advance, zeros_state, (block_decay, block_states))
    device_decay = jnp.exp(jnp.sum(ending, axis=1))
    incoming, passed_decay = prefix(
        (device_state, device_decay),
        "ep",
        combine_states,
        (zeros_state, jnp.ones((head_count,), jnp.float32)),
    )
    causal = jnp.arange(BLOCK)[:, None] >= jnp.arange(BLOCK)[None, :]
    spread = running[:, :, :, None] - running[:, :, None, :]
    weight_table = jnp.exp(jnp.where(causal, spread, -jnp.inf))
    score_matrix = (
        jnp.einsum("nlhd,nmhd->hnlm", query_rot, key_rot, precision=largest_entry) * weight_table
    )
    inside = jnp.einsum("hnlm,nmhe->nlhe", score_matrix, value_all, precision=largest_entry)
    before = jnp.exp(jnp.cumsum(ending, axis=1) - ending)
    starts = local_starts + before.T[:, :, None, None] * incoming[None]
    outside = jnp.einsum(
        "nlhd,hnl,nhde->nlhe", query_rot, jnp.exp(running), starts, precision=largest_entry
    )
    mixed = (inside + outside).reshape(length, head_count, value_width)
    centered = mixed - jnp.mean(mixed, axis=-1, keepdims=True)
    normed = (
        centered
        * lax.rsqrt(jnp.mean(centered * centered, axis=-1, keepdims=True) + epsilon)
        * head_gain.reshape(head_count, value_width)
    )
    return (
        jax.nn.silu(gate_rows.astype(jnp.float32))
        * normed.reshape(length, head_count * value_width)
    ).astype(jnp.bfloat16)


def body(
    queries,
    key_rows,
    value_rows,
    gate_rows,
    log_decay,
    head_gain,
    out_weight,
    expert_input,
    input_gain,
    route_ids,
    route_weight,
    expert_gate,
    expert_up,
    expert_down,
):
    hidden = retention_rows(queries, key_rows, value_rows, gate_rows, log_decay, head_gain)
    tp_count = lax.axis_size("tp")
    model_width = out_weight.shape[1]
    mixer_out = lax.psum_scatter(
        jnp.dot(hidden, out_weight, preferred_element_type=jnp.float32).astype(jnp.bfloat16),
        "tp",
        scatter_dimension=0,
        tiled=True,
    )
    token_count = expert_input.shape[0]
    local_experts = expert_gate.shape[0]
    ep_count = lax.axis_size("ep")
    expert_count = ep_count * local_experts
    capacity = 3 * token_count // expert_count
    quarter = model_width // tp_count
    widened = expert_input.astype(jnp.float32)
    normed = (
        widened
        * lax.rsqrt(jnp.mean(widened * widened, axis=-1, keepdims=True) + epsilon)
        * input_gain
    ).astype(jnp.bfloat16)
    flat_ids = route_ids.reshape(-1)
    matches = (flat_ids[:, None] == jnp.arange(expert_count, dtype=jnp.int32)[None, :]).astype(
        jnp.int32
    )
    slot_rank = jnp.sum((jnp.cumsum(matches, axis=0) - matches) * matches, axis=1)
    target = flat_ids * capacity + slot_rank
    owners = jnp.arange(2 * token_count, dtype=jnp.int32) // 2
    slot_table = jnp.full((expert_count * capacity,), token_count, jnp.int32).at[target].set(owners)
    padded = jnp.concatenate([normed, jnp.zeros((1, model_width), jnp.bfloat16)], axis=0)
    share = capacity // tp_count
    own_slots = lax.dynamic_slice_in_dim(
        slot_table.reshape(expert_count, capacity), lax.axis_index("tp") * share, share, 1
    )
    outgoing = padded[own_slots]
    arrived = lax.all_to_all(outgoing, "ep", split_axis=0, concat_axis=0, tiled=True).reshape(
        ep_count, local_experts, share, model_width
    )
    gate_whole, up_whole, down_whole = (
        lax.all_gather(expert_gate, "tp", axis=2, tiled=True),
        lax.all_gather(expert_up, "tp", axis=2, tiled=True),
        lax.all_gather(expert_down, "tp", axis=1, tiled=True),
    )
    gate_val = jnp.einsum("sxcd,xdf->sxcf", arrived, gate_whole, preferred_element_type=jnp.float32)
    up_val = jnp.einsum("sxcd,xdf->sxcf", arrived, up_whole, preferred_element_type=jnp.float32)
    inner_rows = (jax.nn.silu(gate_val) * up_val).astype(jnp.bfloat16)
    unit_group = expert_down.shape[1]
    group_parts = jnp.einsum(
        "sxcgf,xgfd->gsxcd",
        inner_rows.reshape(ep_count, local_experts, share, tp_count, unit_group),
        down_whole.reshape(local_experts, tp_count, unit_group, model_width),
        preferred_element_type=jnp.float32,
    )
    finished = jnp.sum(round_back(group_parts), axis=0).astype(jnp.bfloat16)
    came_back = lax.all_to_all(finished, "ep", split_axis=0, concat_axis=0, tiled=True)
    returned = lax.all_to_all(came_back, "tp", split_axis=3, concat_axis=2, tiled=True).reshape(
        expert_count * capacity, quarter
    )
    picked = returned[target].reshape(token_count, 2, quarter).astype(jnp.float32)
    expert_out = jnp.sum(picked * route_weight[:, :, None], axis=1).astype(jnp.bfloat16)
    return (mixer_out, expert_out)


def solution(mesh):
    placed = (
        P("ep", "tp"),
        P("ep", "tp"),
        P("ep", "tp"),
        P("ep", "tp"),
        P("tp", "ep"),
        P("tp"),
        P("tp", None),
        P("ep", None),
        P(),
        P("ep", None),
        P("ep", None),
        P("ep", None, "tp"),
        P("ep", None, "tp"),
        P("ep", "tp", None),
    )
    return jax.shard_map(
        body,
        mesh=mesh,
        in_specs=placed,
        out_specs=(P(("ep", "tp"), None), P("ep", "tp")),
        check_vma=False,
    )
```

profile of v0, /device:TPU:0, one launch (start us, length us, event | category | flops | bytes accessed | tf_op | source)
XLA Modules:
  0.0 503.5 jit_solution(17845343262958947994)
XLA Ops:
  18.2 4.1 multiply_subtract_fusion
  22.3 3.2 fusion.36
  28.2 2.3 reduce-window.16
  31.4 4.8 scatter_custom_fusion
  38.1 3.1 fusion.1
  42.8 2.5 concatenate.14
  45.3 11.0 %gather_fusion = bf16[384,4096]{1,0:T(8,128)(2,1)} fusion(bf16[513,4096]{1,0:T(8,128)(2,1)} %concatenate.14, s32[1024]{0:T(1024)S(1)} %pad_clamp_fusion), kind=kCustom, calls=%fused_computation | custom fusion | bytes 6292992 | tf_op jit(solution)/shard_map/gather | solution.py:176
  56.6 7.2 %all-to-all-start = ((bf16[8,48,4096]{2,1,0:T(8,128)(2,1)}), bf16[8,48,4096]{2,1,0:T(8,128)(2,1)}, u32[]{:S(2)}, u32[]{:S(2)}) async-start(bf16[8,48,4096]{2,1,0:T(8,128)(2,1)} %bitcast.27), calls=%async_computation.1 | async-start | bytes 6291456 | tf_op jit(solution)/shard_map/all_to_all | solution.py:177
  63.8 74.4 %all-reduce.1 = bf16[32]{0:T(256)(128)(2,1)S(1)} all-reduce(bf16[32]{0:T(256)(128)(2,1)S(1)} %dynamic-update-slice), channel_id=2, replica_groups=mesh['ep'=8,'tp'=4] {'ep'}, use_global_device_ids=true, to_apply=%add.1 | all-reduce | flops 32 | bytes 128
  138.5 5.4 %fusion.50 = f32[4,512,512]{2,1,0:T(8,128)S(1)} fusion(f32[512,4,64]{2,0,1:T(8,128)} %get-tuple-element.148, f32[512,4,64]{2,0,1:T(8,128)} %get-tuple-element.149, f32[512,4,64]{2,0,1:T(8,128)S(1)} %get-tuple-element.145, f32[512,4,64]{2,0,1:T(8,128)S(1)} %get-tuple-element.144), kind=kOutput, calls=%fused_computation.70 | convolution fusion | flops 1611399168 | bytes 6291456 | tf_op jit(solution)/shard_map/nlhd,nmhd->hnlm/dot_general | solution.py:105
  143.9 4.6 fusion.8
  148.5 9.1 %while.9 = (s32[]{:T(128)}, f32[4,128,256]{2,1,0:T(8,128)S(1)}, s32[]{:T(128)}, bf16[8,4]{1,0:T(8,128)(2,1)S(1)}, bf16[8,4,128,256]{3,2,1,0:T(8,128)(2,1)}, /*index=5*/s32[]{:T(128)}, s32[]{:T(128)}) while((s32[]{:T(128)}, f32[4,128,256]{2,1,0:T(8,128)S(1)}, s32[]{:T(128)}, bf16[8,4]{1,0:T(8,128)(2,1)S(1)}, ...), condition=%wide.region_3.4_spmd.clone, body=%wide.region_2.3_spmd.clone.sunk | while | flops 655368 | bytes 1310865 | solution.py:32
  157.6 4.9 fusion.71
  166.9 2.9 copy.84
  171.8 12.7 %convolution_convert_fusion = bf16[512,4096]{1,0:T(8,128)(2,1)} fusion(bf16[1024,4096]{1,0:T(8,128)(2,1)} %param.22, f32[512,1024]{1,0:T(8,128)} %bitcast.162, f32[512,1024]{1,0:T(8,128)} %copy.83, f32[512,1024]{1,0:T(8,128)} %copy.84, bf16[512,1024]{1,0:T(8,128)(2,1)} %param.19, f32[1024]{0:T(1024)S(1)} %copy-done.7), kind=kOutput, calls=%fused_computation.16 | convolution fusion | flops 4302307328 | bytes 19927040 | tf_op jit(solution)/shard_map/dot_general | solution.py:146
  184.6 7.2 %fusion.6 = f32[8,48,1024]{2,1,0:T(8,128)S(1)} fusion(bf16[8,48,4096]{2,1,0:T(8,128)(2,1)} %all-to-all-done, bf16[1,4096,1024]{2,1,0:T(8,128)(2,1)} %all-gather.7.cloned.1.call-done), kind=kOutput, calls=%fused_computation.14 | convolution fusion | flops 3221225472 | bytes 13107200 | tf_op jit(solution)/shard_map/sxcd,xdf->sxcf/dot_general | solution.py:185
  191.8 41.9 %all-gather.9.cloned.1.call-done = bf16[1,4096,1024]{2,1,0:T(8,128)(2,1)} async-done(((bf16[1,4096,256]{2,1,0:T(8,128)(2,1)}), bf16[1,4096,1024]{2,1,0:T(8,128)(2,1)}) %all-gather.9.cloned.1.call-update) | async-done | bytes 8388624 | tf_op jit(solution)/shard_map/all_gather | solution.py:182
  233.6 7.9 %fusion.27 = bf16[8,1,48,1024]{3,2,0,1:T(8,128)(2,1)S(1)} fusion(f32[8,48,1024]{2,1,0:T(8,128)S(1)} %fusion.6, bf16[8,48,4096]{2,1,0:T(8,128)(2,1)} %all-to-all-done, bf16[1,4096,1024]{2,1,0:T(8,128)(2,1)} %all-gather.9.cloned.1.call-done), kind=kOutput, calls=%fused_computation.42 | convolution fusion | flops 3223584768 | bytes 13893632 | tf_op jit(solution)/shard_map/sxcd,xdf->sxcf/dot_general | solution.py:186
  242.1 51.3 %all-gather.11.cloned.1.call-done = bf16[1,1024,4096]{2,1,0:T(8,128)(2,1)} async-done(((bf16[1,256,4096]{2,1,0:T(8,128)(2,1)}), bf16[1,1024,4096]{2,1,0:T(8,128)(2,1)}) %all-gather.11.cloned.1.call-update) | async-done | bytes 8388624 | tf_op jit(solution)/shard_map/all_gather | solution.py:183
  293.3 10.3 %convert_bitcast_fusion = bf16[4,8,1,48,4096]{4,3,1,0,2:T(8,128)(2,1)} fusion(bf16[4,256,4096,1]{2,1,3,0:T(8,128)(2,1)} %bitcast.159, bf16[8,48,4,256]{3,2,1,0:T(4,128)(2,1)S(1)} %reshape.414), kind=kOutput, calls=%fused_computation.6 | convolution fusion | flops 3227516928 | bytes 21757952 | tf_op jit(solution)/shard_map/sxcgf,xgfd->gsxcd/dot_general | solution.py:189
  303.6 8.6 %reduce_sum.70 = bf16[8,48,4096]{2,1,0:T(8,128)(2,1)S(1)} reduce(bf16[4,8,1,48,4096]{4,3,1,0,2:T(8,128)(2,1)} %convert_bitcast_fusion, bf16[]{:T(256)} %constant.105.clone.1), dimensions={0,2}, to_apply=%region_12.13 | reduce | flops 4718592 | bytes 15728642 | tf_op jit(solution)/shard_map/reduce_sum | solution.py:195
  312.2 76.6 %all_to_all.25 = bf16[8,1,48,4096]{3,2,1,0:T(8,128)(2,1)} all-to-all(bf16[8,1,48,4096]{3,2,1,0:T(8,128)(2,1)S(1)} %bitcast.155), channel_id=1, replica_groups=mesh['ep'=8,'tp'=4] {'ep'}, dimensions={0} | all-to-all | bytes 6291456 | tf_op jit(solution)/shard_map/all_to_all | solution.py:196
  388.8 9.7 %copy.90 = bf16[8,1,48,4096]{2,0,1,3:T(8,128)(2,1)} copy(bf16[8,1,48,4096]{3,2,1,0:T(8,128)(2,1)} %all_to_all.25) | data formatting | bytes 6291456 | tf_op jit(solution)/shard_map/all_to_all | solution.py:196
  398.5 14.8 %reshape.467 = bf16[4,2,196608]{2,1,0:T(2,128)(2,1)} reshape(bf16[4096,1,8,48]{3,2,1,0:T(8,128)(2,1)} %bitcast.152) | data formatting | bytes 6291456
  413.3 4.0 all-to-all-start.2
  417.5 36.7 %all-to-all-done.2 = bf16[4,2,196608]{2,1,0:T(2,128)(2,1)S(1)} async-done(((bf16[4,2,196608]{2,1,0:T(2,128)(2,1)}), bf16[4,2,196608]{2,1,0:T(2,128)(2,1)S(1)}, u32[]{:S(2)}, u32[]{:S(2)}) %all-to-all-start.2) | async-done | bytes 3145760 | tf_op jit(solution)/shard_map/all_to_all | solution.py:197
  454.2 9.9 %reshape.468 = bf16[4096,1,8,48]{3,2,1,0:T(8,128)(2,1)} reshape(bf16[4,2,196608]{2,1,0:T(2,128)(2,1)S(1)} %all-to-all-done.2) | data formatting | bytes 6291456
  464.1 10.2 %copy.99 = bf16[8,1,48,4,1024]{4,3,2,0,1:T(4,128)(2,1)} copy(bf16[8,1,48,4,1024]{2,0,4,3,1:T(8,128)(2,1)} %bitcast.153) | data formatting | bytes 6291456 | tf_op jit(solution)/shard_map/all_to_all | solution.py:197
  474.3 3.0 copy.92
  477.3 5.4 %gather_fusion.1 = bf16[1024,1024]{1,0:T(8,128)(2,1)} fusion(bf16[1536,1024]{1,0:T(8,128)(2,1)S(1)} %bitcast.151, s32[1024]{0:T(1024)S(1)} %broadcast_clamp_fusion), kind=kCustom, calls=%fused_computation.1 | custom fusion | bytes 4198400 | tf_op jit(solution)/shard_map/gather | solution.py:200
  482.7 5.4 %reshape.423 = f32[512,2,1024]{2,1,0:T(2,128)} reshape(bf16[1024,1024]{1,0:T(8,128)(2,1)} %gather_fusion.1) | data formatting | bytes 6291456 | tf_op jit(solution)/shard_map/convert_element_type | solution.py:200
  488.2 8.6 %multiply_reduce_fusion = bf16[512,1024]{1,0:T(8,128)(2,1)} fusion(f32[512,2,1024]{2,1,0:T(2,128)} %reshape.423, f32[512,2]{1,0:T(8,128)S(1)} %copy.93), kind=kLoop, calls=%fused_computation.17 | loop fusion | flops 1572864 | bytes 5246976 | tf_op jit(solution)/shard_map/reduce_sum | solution.py:201
  (108 shorter events, 33.3 us)
Async XLA Ops:
  7.2 141.3 %all-gather.13.cloned.1.call-start = ((), (), s32[]{:S(2)}) async-start(), calls=%async_computation.8 | async-start | bytes 2359296 | tf_op jit(solution)/shard_map/all_gather | solution.py:15
  9.5 4.2 copy-start.3
  18.2 4.1 copy-start.1
  25.5 2.1 copy-start.5
  25.5 159.0 %all-gather.7.cloned.1.call-start = ((), (), s32[]{:S(2)}) async-start(), calls=%async_computation.5 | async-start | bytes 10485760 | tf_op jit(solution)/shard_map/all_gather | solution.py:181
  26.3 10.1 %copy-start.8 = (u32[32]{0:T(128)S(1)}, u32[32]{0:T(128)}, u32[]{:S(2)}) copy-start(u32[32]{0:T(128)} %constant.120) | copy-start | bytes 388
  26.3 207.3 %all-gather.9.cloned.1.call-start = ((), (), s32[]{:S(2)}) async-start(), calls=%async_computation.6 | async-start | bytes 10485760 | tf_op jit(solution)/shard_map/all_gather | solution.py:182
  27.0 266.3 %all-gather.11.cloned.1.call-start = ((), (), s32[]{:S(2)}) async-start(), calls=%async_computation.7 | async-start | bytes 10485760 | tf_op jit(solution)/shard_map/all_gather | solution.py:183
  27.6 13.5 %copy-start.4 = (f32[4096]{0:T(1024)S(1)}, f32[4096]{0:T(1024)}, u32[]{:S(2)}) copy-start(f32[4096]{0:T(1024)} %param.24) | copy-start | bytes 49156
  36.4 4.7 copy-start
  56.6 128.0 %all-to-all-start = ((bf16[8,48,4096]{2,1,0:T(8,128)(2,1)}), bf16[8,48,4096]{2,1,0:T(8,128)(2,1)}, u32[]{:S(2)}, u32[]{:S(2)}) async-start(bf16[8,48,4096]{2,1,0:T(8,128)(2,1)} %bitcast.27), calls=%async_computation.1 | async-start | bytes 6291456 | tf_op jit(solution)/shard_map/all_to_all | solution.py:177
  63.8 433.0 %reduce-scatter.2.cloned.1.call-start = ((), (), s32[]{:S(2)}) async-start(), calls=%async_computation.4 | async-start | bytes 5242880 | tf_op jit(solution)/shard_map/reduce_scatter | solution.py:145
  138.5 5.5 %copy-start.2 = (bf16[512,1024]{1,0:T(8,128)(2,1)S(1)}, bf16[512,1024]{1,0:T(8,128)(2,1)}, u32[]{:S(2)}) copy-start(bf16[512,1024]{1,0:T(8,128)(2,1)} %param.18) | copy-start | bytes 3145732
  169.8 2.0 copy-start.7
  413.3 4.0 copy-start.6
  413.3 40.9 %all-to-all-start.2 = ((bf16[4,2,196608]{2,1,0:T(2,128)(2,1)}), bf16[4,2,196608]{2,1,0:T(2,128)(2,1)S(1)}, u32[]{:S(2)}, u32[]{:S(2)}) async-start(bf16[4,2,196608]{2,1,0:T(2,128)(2,1)} %reshape.467), calls=%async_computation.3 | async-start | bytes 6291456 | tf_op jit(solution)/shard_map/all_to_all | solution.py:197
Sparse Core Ops, SparseCore 0:
  25.7 72.0 all-gather.12
  99.3 73.3 all-gather.6
  174.2 59.3 all-gather.8
  235.0 58.2 all-gather.10
  296.3 44.5 reduce-scatter.1
where the time goes:
time: 511 us; the launch traced here: 503 us
  blocking collectives  151 us (30%)
  waiting for transfers between devices  132 us (26%)
  local copies, waits for them, and re-layouts  97.1 us (19%)
  matrix products  56.1 us (11%)
  other arithmetic  40.3 us (8%)
  between operations  15.4 us (3%)
  starting transfers between devices  11.4 us (2%)
    all_to_all x1, blocking collectives, body(): lax.all_to_all(finished, 'ep', split_axis=0, concat_axis=0, tiled=True)  76.6 us
    unnamed x1, blocking collectives  74.4 us
    all_gather x1, waiting for transfers between devices, body(): lax.all_gather(expert_down, 'tp', axis=1, tiled=True)  51.3 us
    all_gather x1, waiting for transfers between devices, body(): lax.all_gather(expert_up, 'tp', axis=2, tiled=True)  41.9 us
    all_to_all x1, waiting for transfers between devices, body(): lax.all_to_all(came_back, 'tp', split_axis=3, concat_axis=2, tiled=True)  36.7 us
    unnamed x32, local copies, waits for them, and re-layouts  34.6 us
    all_to_all x2, local copies, waits for them, and re-layouts, body(): lax.all_to_all(came_back, 'tp', split_axis=3, concat_axis=2, tiled=True)  13.2 us
    dot_general x1, matrix products, body(): jnp.dot(hidden, out_weight, preferred_element_type=jnp.float32)  12.7 us
  transfers between devices with their start and end apart: 7, of which 3 were waited for; matrix products, arithmetic and copies ran while one was open for 35% of the time, Pallas kernels for 0%

commit v1 on v0

--- a/solution.py
+++ b/solution.py
@@ -194,9 +194,16 @@
     )
     finished = jnp.sum(round_back(group_parts), axis=0).astype(jnp.bfloat16)
     came_back = lax.all_to_all(finished, "ep", split_axis=0, concat_axis=0, tiled=True)
-    returned = lax.all_to_all(came_back, "tp", split_axis=3, concat_axis=2, tiled=True).reshape(
-        expert_count * capacity, quarter
-    )
+    set_the_positions = lambda w_in: jnp.concatenate(
+        jax.lax.all_to_all(
+            jnp.stack(jnp.split(w_in, jax.lax.axis_size("tp"), axis=3), axis=0),
+            axis_name="tp",
+            split_axis=0,
+            concat_axis=0,
+        ),
+        axis=2,
+    )
+    returned = set_the_positions(came_back).reshape(expert_count * capacity, quarter)
     picked = returned[target].reshape(token_count, 2, quarter).astype(jnp.float32)
     expert_out = jnp.sum(picked * route_weight[:, :, None], axis=1).astype(jnp.bfloat16)
     return (mixer_out, expert_out)

time: 511 us -> 471 us (0.922)
  blocking collectives: 151 us -> 74.5 us
  waiting for transfers between devices: 132 us -> 204 us
  local copies, waits for them, and re-layouts: 97.1 us -> 53.8 us
  starting transfers between devices: 11.4 us -> 17.3 us
    all_to_all x1 -> x0, blocking collectives: 76.6 us -> none  [body(): lax.all_to_all(finished, 'ep', split_axis=0, concat_axis=0, tiled=True)]
    all_to_all x1 -> x2, waiting for transfers between devices: 36.7 us -> 95.2 us  [the longest x1 58.5 us: body(): lax.all_to_all(finished, 'ep', split_axis=0, concat_axis=0, tiled=True)]
    all_to_all x3 -> x0, local copies, waits for them, and re-layouts: 22.9 us -> none  [the longest x2 13.2 us: body(): lax.all_to_all(came_back, 'tp', split_axis=3, concat_axis=2, tiled=True)]
    unnamed x32, local copies, waits for them, and re-layouts: 34.6 us -> 11.8 us
    all_gather x1, waiting for transfers between devices: 41.9 us -> 54 us  [body(): lax.all_gather(expert_up, 'tp', axis=2, tiled=True)]
    all_to_all x1 -> x2, starting transfers between devices: 4 us -> 9.48 us  [the longest x1 5.65 us: body(): lax.all_to_all(finished, 'ep', split_axis=0, concat_axis=0, tiled=True)]
  transfers between devices with their start and end apart: 7 -> 8, of which waited for: 3 -> 5; matrix products, arithmetic and copies ran while one was open for 35% -> 24% of each run, Pallas kernels for 0% -> 0%
where the time goes in v1:
time: 471 us; the launch traced here: 464 us
  waiting for transfers between devices  204 us (43%)
  blocking collectives  74.5 us (16%)
  matrix products  55.1 us (12%)
  local copies, waits for them, and re-layouts  53.8 us (11%)
  other arithmetic  43.6 us (9%)
  starting transfers between devices  17.3 us (4%)
  between operations  15.2 us (3%)
    unnamed x1, blocking collectives  74.5 us
    all_to_all x1, waiting for transfers between devices, body(): lax.all_to_all(finished, 'ep', split_axis=0, concat_axis=0, tiled=True)  58.5 us
    all_gather x1, waiting for transfers between devices, body(): lax.all_gather(expert_up, 'tp', axis=2, tiled=True)  54 us
    all_gather x1, waiting for transfers between devices, body(): lax.all_gather(expert_down, 'tp', axis=1, tiled=True)  51.1 us
    all_to_all x1, waiting for transfers between devices, body(): jax.lax.all_to_all(jnp.stack(jnp.split(w_in, jax.lax.axis_size('tp'), axi...  36.7 us
    dot_general x1, matrix products, body(): jnp.dot(hidden, out_weight, preferred_element_type=jnp.float32)  12.3 us
    unnamed x32, local copies, waits for them, and re-layouts  11.8 us
    gather x1, local copies, waits for them, and re-layouts, body(): outgoing = padded[own_slots]  11 us
  transfers between devices with their start and end apart: 8, of which 5 were waited for; matrix products, arithmetic and copies ran while one was open for 24% of the time, Pallas kernels for 0%

profile of v1, /device:TPU:0, one launch (start us, length us, event | category | flops | bytes accessed | tf_op | source)
XLA Modules:
  0.0 463.6 jit_solution(15630380015831466625)
XLA Ops:
  18.2 4.1 multiply_subtract_fusion
  22.3 3.2 fusion.36
  28.1 2.3 reduce-window.16
  31.3 4.8 %scatter_custom_fusion = s32[1536]{0:T(1024)S(1)} fusion(s32[1024]{0:T(1024)S(1)} %bitcast.179, s32[1024]{0:T(1024)S(1)} %add_select_fusion, s32[]{:T(128)} %constant.95.clone.1), kind=kCustom, calls=%fused_computation.99 | custom fusion | bytes 6148 | tf_op jit(solution)/shard_map/scatter | solution.py:170
  36.4 3.3 fusion.1
  41.6 2.5 concatenate.14
  44.0 11.0 %gather_fusion = bf16[384,4096]{1,0:T(8,128)(2,1)} fusion(bf16[513,4096]{1,0:T(8,128)(2,1)} %concatenate.14, s32[1024]{0:T(1024)S(1)} %pad_clamp_fusion), kind=kCustom, calls=%fused_computation | custom fusion | bytes 6292992 | tf_op jit(solution)/shard_map/gather | solution.py:176
  55.0 7.4 %all-to-all-start = ((bf16[8,48,4096]{2,1,0:T(8,128)(2,1)}), bf16[8,48,4096]{2,1,0:T(8,128)(2,1)}, u32[]{:S(2)}, u32[]{:S(2)}) async-start(bf16[8,48,4096]{2,1,0:T(8,128)(2,1)} %bitcast.27), calls=%async_computation.1 | async-start | bytes 6291456 | tf_op jit(solution)/shard_map/all_to_all | solution.py:177
  63.9 74.5 %all-reduce.1 = bf16[32]{0:T(256)(128)(2,1)S(1)} all-reduce(bf16[32]{0:T(256)(128)(2,1)S(1)} %dynamic-update-slice), channel_id=2, replica_groups=mesh['ep'=8,'tp'=4] {'ep'}, use_global_device_ids=true, to_apply=%add.1 | all-reduce | flops 32 | bytes 128
  138.6 5.4 %fusion.50 = f32[4,512,512]{2,1,0:T(8,128)S(1)} fusion(f32[512,4,64]{2,0,1:T(8,128)} %get-tuple-element.151, f32[512,4,64]{2,0,1:T(8,128)} %get-tuple-element.152, f32[512,4,64]{2,0,1:T(8,128)S(1)} %get-tuple-element.148, f32[512,4,64]{2,0,1:T(8,128)S(1)} %get-tuple-element.147), kind=kOutput, calls=%fused_computation.75 | convolution fusion | flops 1611399168 | bytes 6291456 | tf_op jit(solution)/shard_map/nlhd,nmhd->hnlm/dot_general | solution.py:105
  144.0 4.6 fusion.8
  148.6 9.1 %while.9 = (s32[]{:T(128)}, f32[4,128,256]{2,1,0:T(8,128)S(1)}, s32[]{:T(128)}, bf16[8,4]{1,0:T(8,128)(2,1)S(1)}, bf16[8,4,128,256]{3,2,1,0:T(8,128)(2,1)}, /*index=5*/s32[]{:T(128)}, s32[]{:T(128)}) while((s32[]{:T(128)}, f32[4,128,256]{2,1,0:T(8,128)S(1)}, s32[]{:T(128)}, bf16[8,4]{1,0:T(8,128)(2,1)S(1)}, ...), condition=%wide.region_3.4_spmd.clone, body=%wide.region_2.3_spmd.clone.sunk | while | flops 655368 | bytes 1310865 | solution.py:32
  157.6 4.9 %fusion.71 = (f32[512,4]{0,1:T(4,128)S(1)}, f32[1,512,4,256]{1,3,2,0:T(8,128)S(1)}) fusion(f32[4,128,256]{2,1,0:T(8,128)S(1)} %get-tuple-element.111, f32[4]{0:T(128)S(1)} %get-tuple-element.140, f32[4,512]{1,0:T(4,128)S(1)} %get-tuple-element.142, f32[512,4,64]{2,0,1:T(8,128)} %get-tuple-element.151, f32[512,4,64]{2,0,1:T(8,128)} %get-tuple-element.152, ...), kind=kOutput, calls=%fused_computation.123 | convolution fusion | flops 807008256 | bytes 5783568 | tf_op jit(solution)/shard_map/nlhd,hnl,nhde->nlhe/dot_general | solution.py:110
  163.6 1.8 copy.112
  167.0 2.9 copy.90
  169.9 1.9 copy.89
  173.4 7.0 %fusion.6 = f32[8,48,1024]{2,1,0:T(8,128)S(1)} fusion(bf16[8,48,4096]{2,1,0:T(8,128)(2,1)} %all-to-all-done, bf16[1,4096,1024]{2,1,0:T(8,128)(2,1)} %all-gather.7.cloned.1.call-done), kind=kOutput, calls=%fused_computation.14 | convolution fusion | flops 3221225472 | bytes 13107200 | tf_op jit(solution)/shard_map/sxcd,xdf->sxcf/dot_general | solution.py:185
  180.4 54.0 %all-gather.9.cloned.1.call-done = bf16[1,4096,1024]{2,1,0:T(8,128)(2,1)} async-done(((bf16[1,4096,256]{2,1,0:T(8,128)(2,1)}), bf16[1,4096,1024]{2,1,0:T(8,128)(2,1)}) %all-gather.9.cloned.1.call-update) | async-done | bytes 8388624 | tf_op jit(solution)/shard_map/all_gather | solution.py:182
  234.4 8.0 %fusion.27 = bf16[8,1,48,1024]{3,2,0,1:T(8,128)(2,1)S(1)} fusion(f32[8,48,1024]{2,1,0:T(8,128)S(1)} %fusion.6, bf16[8,48,4096]{2,1,0:T(8,128)(2,1)} %all-to-all-done, bf16[1,4096,1024]{2,1,0:T(8,128)(2,1)} %all-gather.9.cloned.1.call-done), kind=kOutput, calls=%fused_computation.43 | convolution fusion | flops 3223584768 | bytes 13893632 | tf_op jit(solution)/shard_map/sxcd,xdf->sxcf/dot_general | solution.py:186
  243.0 51.1 %all-gather.11.cloned.1.call-done = bf16[1,1024,4096]{2,1,0:T(8,128)(2,1)} async-done(((bf16[1,256,4096]{2,1,0:T(8,128)(2,1)}), bf16[1,1024,4096]{2,1,0:T(8,128)(2,1)}) %all-gather.11.cloned.1.call-update) | async-done | bytes 8388624 | tf_op jit(solution)/shard_map/all_gather | solution.py:183
  294.1 9.8 %convert_bitcast_fusion = bf16[4,8,1,48,4096]{4,3,1,0,2:T(8,128)(2,1)} fusion(bf16[4,256,4096,1]{2,1,3,0:T(8,128)(2,1)} %bitcast.166, bf16[8,48,4,256]{3,2,1,0:T(4,128)(2,1)S(1)} %reshape.413), kind=kOutput, calls=%fused_computation.6 | convolution fusion | flops 3227516928 | bytes 21757952 | tf_op jit(solution)/shard_map/sxcgf,xgfd->gsxcd/dot_general | solution.py:189
  303.9 9.7 %reduce_sum.70 = bf16[8,48,4096]{2,1,0:T(8,128)(2,1)} reduce(bf16[4,8,1,48,4096]{4,3,1,0,2:T(8,128)(2,1)} %convert_bitcast_fusion, bf16[]{:T(256)} %constant.105.clone.1), dimensions={0,2}, to_apply=%region_12.13 | reduce | flops 4718592 | bytes 15728642 | tf_op jit(solution)/shard_map/reduce_sum | solution.py:195
  313.6 5.6 %all-to-all-start.1 = ((bf16[8,1,48,4096]{3,2,1,0:T(8,128)(2,1)}), bf16[8,1,48,4096]{3,2,1,0:T(8,128)(2,1)S(1)}, u32[]{:S(2)}, u32[]{:S(2)}) async-start(bf16[8,1,48,4096]{3,2,1,0:T(8,128)(2,1)} %bitcast.163), calls=%async_computation.2 | async-start | bytes 6291456 | tf_op jit(solution)/shard_map/all_to_all | solution.py:196
  319.6 12.3 %convolution_convert_fusion = bf16[512,4096]{1,0:T(8,128)(2,1)} fusion(bf16[1024,4096]{1,0:T(8,128)(2,1)} %param.22, f32[512,1024]{1,0:T(8,128)} %bitcast.169, f32[512,1024]{1,0:T(8,128)} %copy.89, f32[512,1024]{1,0:T(8,128)} %copy.90, bf16[512,1024]{1,0:T(8,128)(2,1)} %param.19, f32[1024]{0:T(1024)S(1)} %copy-done.8), kind=kOutput, calls=%fused_computation.16 | convolution fusion | flops 4302307328 | bytes 19927040 | tf_op jit(solution)/shard_map/dot_general | solution.py:146
  331.9 58.5 %all-to-all-done.1 = bf16[8,1,48,4096]{3,2,1,0:T(8,128)(2,1)S(1)} async-done(((bf16[8,1,48,4096]{3,2,1,0:T(8,128)(2,1)}), bf16[8,1,48,4096]{3,2,1,0:T(8,128)(2,1)S(1)}, u32[]{:S(2)}, u32[]{:S(2)}) %all-to-all-start.1) | async-done | bytes 3145760 | tf_op jit(solution)/shard_map/all_to_all | solution.py:196
  390.7 1.9 pad_maximum_fusion
  392.6 3.8 all-to-all-start.2
  396.6 36.7 %all-to-all-done.2 = bf16[4,8,1,48,1024]{4,3,1,2,0:T(8,128)(2,1)S(1)} async-done(((bf16[4,8,1,48,1024]{4,3,1,2,0:T(8,128)(2,1)}), bf16[4,8,1,48,1024]{4,3,1,2,0:T(8,128)(2,1)S(1)}, u32[]{:S(2)}, u32[]{:S(2)}) %all-to-all-start.2) | async-done | bytes 3145760 | tf_op jit(solution)/shard_map/all_to_all | solution.py:198
  435.0 2.3 copy.99
  437.3 5.4 %gather_fusion.1 = bf16[1024,1024]{1,0:T(8,128)(2,1)} fusion(bf16[1536,1024]{1,0:T(8,128)(2,1)S(1)} %bitcast.159, s32[1024]{0:T(1024)S(1)} %broadcast_clamp_fusion), kind=kCustom, calls=%fused_computation.1 | custom fusion | bytes 4198400 | tf_op jit(solution)/shard_map/gather | solution.py:207
  442.7 5.4 %reshape.422 = f32[512,2,1024]{2,1,0:T(2,128)} reshape(bf16[1024,1024]{1,0:T(8,128)(2,1)} %gather_fusion.1) | data formatting | bytes 6291456 | tf_op jit(solution)/shard_map/convert_element_type | solution.py:207
  448.1 8.6 %multiply_reduce_fusion = bf16[512,1024]{1,0:T(8,128)(2,1)} fusion(f32[512,2,1024]{2,1,0:T(2,128)} %reshape.422, f32[512,2]{1,0:T(8,128)S(1)} %copy.100), kind=kLoop, calls=%fused_computation.17 | loop fusion | flops 1572864 | bytes 5246976 | tf_op jit(solution)/shard_map/reduce_sum | solution.py:208
  (110 shorter events, 33.6 us)
Async XLA Ops:
  7.2 141.4 %all-gather.13.cloned.1.call-start = ((), (), s32[]{:S(2)}) async-start(), calls=%async_computation.8 | async-start | bytes 2359296 | tf_op jit(solution)/shard_map/all_gather | solution.py:15
  9.5 4.2 copy-start.4
  18.2 4.1 copy-start.2
  25.5 2.1 copy-start.6
  25.5 147.9 %all-gather.7.cloned.1.call-start = ((), (), s32[]{:S(2)}) async-start(), calls=%async_computation.5 | async-start | bytes 10485760 | tf_op jit(solution)/shard_map/all_gather | solution.py:181
  26.3 208.1 %all-gather.9.cloned.1.call-start = ((), (), s32[]{:S(2)}) async-start(), calls=%async_computation.6 | async-start | bytes 10485760 | tf_op jit(solution)/shard_map/all_gather | solution.py:182
  27.0 267.1 %all-gather.11.cloned.1.call-start = ((), (), s32[]{:S(2)}) async-start(), calls=%async_computation.7 | async-start | bytes 10485760 | tf_op jit(solution)/shard_map/all_gather | solution.py:183
  27.6 12.1 %copy-start.5 = (f32[4096]{0:T(1024)S(1)}, f32[4096]{0:T(1024)}, u32[]{:S(2)}) copy-start(f32[4096]{0:T(1024)} %param.24) | copy-start | bytes 49156
  36.4 3.5 copy-start
  55.0 7.4 %copy-start.9 = (u32[32]{0:T(128)S(1)}, u32[32]{0:T(128)}, u32[]{:S(2)}) copy-start(u32[32]{0:T(128)} %constant.120) | copy-start | bytes 388
  55.0 116.7 %all-to-all-start = ((bf16[8,48,4096]{2,1,0:T(8,128)(2,1)}), bf16[8,48,4096]{2,1,0:T(8,128)(2,1)}, u32[]{:S(2)}, u32[]{:S(2)}) async-start(bf16[8,48,4096]{2,1,0:T(8,128)(2,1)} %bitcast.27), calls=%async_computation.1 | async-start | bytes 6291456 | tf_op jit(solution)/shard_map/all_to_all | solution.py:177
  138.6 5.4 %copy-start.3 = (bf16[512,1024]{1,0:T(8,128)(2,1)S(1)}, bf16[512,1024]{1,0:T(8,128)(2,1)}, u32[]{:S(2)}) copy-start(bf16[512,1024]{1,0:T(8,128)(2,1)} %param.18) | copy-start | bytes 3145732
  313.6 5.9 %copy-start.8 = (f32[1024]{0:T(1024)S(1)}, f32[1024]{0:T(1024)}, u32[]{:S(2)}) copy-start(f32[1024]{0:T(1024)} %param.21) | copy-start | bytes 12292
  313.6 76.8 %all-to-all-start.1 = ((bf16[8,1,48,4096]{3,2,1,0:T(8,128)(2,1)}), bf16[8,1,48,4096]{3,2,1,0:T(8,128)(2,1)S(1)}, u32[]{:S(2)}, u32[]{:S(2)}) async-start(bf16[8,1,48,4096]{3,2,1,0:T(8,128)(2,1)} %bitcast.163), calls=%async_computation.2 | async-start | bytes 6291456 | tf_op jit(solution)/shard_map/all_to_all | solution.py:196
  319.3 137.4 %reduce-scatter.2.cloned.1.call-start = ((), (), s32[]{:S(2)}) async-start(), calls=%async_computation.4 | async-start | bytes 5242880 | tf_op jit(solution)/shard_map/reduce_scatter | solution.py:145
  392.6 3.8 copy-start.7
  392.6 40.7 %all-to-all-start.2 = ((bf16[4,8,1,48,1024]{4,3,1,2,0:T(8,128)(2,1)}), bf16[4,8,1,48,1024]{4,3,1,2,0:T(8,128)(2,1)S(1)}, u32[]{:S(2)}, u32[]{:S(2)}) async-start(bf16[4,8,1,48,1024]{4,3,1,2,0:T(8,128)(2,1)} %pad_maximum_fusion), calls=%async_computation.3 | async-start | bytes 6291456 | tf_op jit(solution)/shard_map/all_to_all | solution.py:198
  433.3 1.7 copy-start.1
Sparse Core Ops, SparseCore 0:
  25.7 73.3 all-gather.12
  100.6 72.7 all-gather.6
  175.0 59.3 all-gather.8
  235.8 58.2 all-gather.10
  332.0 45.0 reduce-scatter.1
